TPU v7x, 32 devices: a whole 2x2x4 slice. The times are simulated.
32 devices in a mesh: sp: 8 (over z, x), tp: 4 (over y, core).
Axes of the slice: x: 2, y: 2, z: 4, core: 2. Of those that a mesh axis runs over, the one named last changes fastest.
Arguments:
- queries: bfloat16 [1024, 2048], P('sp', 'tp'), may hold values from -6 to 6
- key_rows: bfloat16 [1024, 2048], P('sp', 'tp'), may hold values from -6 to 6
- value_rows: bfloat16 [1024, 2048], P('sp', 'tp'), may hold values from -6 to 6
- gate_input: bfloat16 [1024, 2048], P('sp', 'tp'), may hold values from -6 to 6
- log_decay: float32 [1024, 16], P('sp', 'tp'), may hold values from -0.6 to 0, as said below
- head_gain: float32 [2048], P('tp'), may hold values from 0.1 to 1.9
- out_weight: bfloat16 [2048, 2048], P('tp'), may hold values from -0.125 to 0.125
- residual: bfloat16 [1024, 2048], P('sp'), may hold values from -6 to 6
- mlp_gain: float32 [2048], replicated, may hold values from 0.1 to 1.9
- gate_weight: bfloat16 [2048, 5632], P('sp', 'tp'), may hold values from -0.125 to 0.125
- up_weight: bfloat16 [2048, 5632], P('sp', 'tp'), may hold values from -0.125 to 0.125
- down_weight: bfloat16 [5632, 2048], P('tp', 'sp'), may hold values from -0.078125 to 0.078125
Outputs:
- layer_out: bfloat16 [1024, 2048], P(('sp', 'tp'))
Inputs may be any that keep to these rules, and one draw needn't show every extreme that they name: log_decay holds the logarithm of a decay factor of each head at each position.
All inputs are finite; a program needn't handle non-finite values.
Results may differ from a plain program's by a relative error of at most 0.017.
Values may be sent and summed in bfloat16 or wider, within the bound.
A program may use at most 128 MiB of HBM per device.

v0:
```python
import jax
import jax.numpy as jnp
from jax import lax
from jax.sharding import PartitionSpec as P

BLOCK = 128
EPS = 1e-06


def prefix_2(x, axis, join, neutral):
    place = lax.axis_index(axis)
    gathered = jax.tree.map(
        lambda a, kind: lax.all_gather(a.astype(kind), axis), x, (jnp.bfloat16, jnp.bfloat16)
    )
    state = jax.tree.map(lambda a, e: jnp.zeros_like(a) + jnp.asarray(e, a.dtype), x, neutral)

    def one(step, state):
        return join(
            state,
            jax.tree.map(
                lambda a, own: lax.dynamic_index_in_dim(a, step, 0, False).astype(own.dtype),
                gathered,
                x,
            ),
        )

    return lax.fori_loop(0, place, one, state)


def rotate(values_in, positions):
    half = values_in.shape[-1] // 2
    freq = 10000.0 ** (-jnp.linspace(0.0, 1.0, half, dtype=jnp.float32))
    angles = positions * freq
    angles = jnp.concatenate([angles, angles], axis=-1)
    first = values_in[..., :half]
    second = values_in[..., half:]
    turned = jnp.concatenate([-second, first], axis=-1)
    return values_in * jnp.cos(angles) + turned * jnp.sin(angles)


def row_norm(stream, gain):
    return stream * lax.rsqrt(jnp.mean(stream * stream, axis=-1, keepdims=True) + EPS) * gain


def join_states(earlier, later):
    return (earlier[0] * later[0], later[0][:, None, None] * earlier[1] + later[1])


def body(
    queries,
    key_rows,
    value_rows,
    gate_input,
    log_decay,
    head_gain,
    out_weight,
    residual,
    mlp_gain,
    gate_weight,
    up_weight,
    down_weight,
):
    tok_rows = queries.shape[0]
    heads_here = log_decay.shape[1]
    head_size = head_gain.shape[0] // heads_here
    quarter = tok_rows // lax.axis_size("tp")
    offset = lax.axis_index("sp") * tok_rows
    positions = (offset + lax.iota(jnp.int32, tok_rows)).astype(jnp.float32)[:, None, None]
    q_rot = rotate(
        queries.reshape(tok_rows, heads_here, head_size).astype(jnp.float32), positions
    ).astype(jnp.bfloat16)
    k_rot = (
        rotate(key_rows.reshape(tok_rows, heads_here, head_size).astype(jnp.float32), positions)
        * head_size ** (-0.5)
    ).astype(jnp.bfloat16)
    blocks = tok_rows // BLOCK
    q_blocks = q_rot.reshape(blocks, BLOCK, heads_here, head_size)
    k_blocks = k_rot.reshape(blocks, BLOCK, heads_here, head_size)
    v_blocks = value_rows.reshape(blocks, BLOCK, heads_here, head_size)
    cumul = jnp.cumsum(log_decay.reshape(blocks, BLOCK, heads_here), axis=1)
    by_head = cumul.transpose(0, 2, 1)
    lower = jnp.tril(jnp.ones((BLOCK, BLOCK), dtype=bool))
    spread = by_head[:, :, :, None] - by_head[:, :, None, :]
    weight = jnp.where(lower, jnp.exp(jnp.where(lower, spread, 0.0)), 0.0)
    scores = jnp.einsum("nthd,nshd->nhts", q_blocks, k_blocks, preferred_element_type=jnp.float32)
    probs = (scores * weight).astype(jnp.bfloat16)
    inner = jnp.einsum("nhts,nshe->nthe", probs, v_blocks, preferred_element_type=jnp.float32)
    k_weighted = (
        k_blocks.astype(jnp.float32) * jnp.exp(cumul[:, -1:, :] - cumul)[..., None]
    ).astype(jnp.bfloat16)
    contrib = jnp.einsum(
        "nshd,nshe->nhde", k_weighted, v_blocks, preferred_element_type=jnp.float32
    )
    totals = jnp.exp(cumul[:, -1, :])

    def advance(carry, items):
        state, prefix = carry
        factor, update = items
        return ((state * factor[:, None, None] + update, prefix * factor), (state, prefix))

    start_state = jnp.zeros((heads_here, head_size, head_size), jnp.float32)
    start_prefix = jnp.ones((heads_here,), jnp.float32)
    (dev_state, dev_total), (local_before, prefixes) = lax.scan(
        advance, (start_state, start_prefix), (totals, contrib)
    )
    _, incoming = prefix_2((dev_total, dev_state), "sp", join_states, (start_prefix, start_state))
    before = local_before + prefixes[:, :, None, None] * incoming[None]
    cross = jnp.einsum(
        "nthd,nhde->nthe", q_blocks.astype(jnp.float32), before, precision=lax.Precision.HIGHEST
    )
    cross = cross * jnp.exp(cumul)[..., None]
    result = (inner + cross).reshape(tok_rows, heads_here, head_size)
    result = row_norm(result, head_gain.reshape(heads_here, head_size)).reshape(
        tok_rows, heads_here * head_size
    )
    retained = (result * jax.nn.silu(gate_input.astype(jnp.float32))).astype(jnp.bfloat16)
    picked = retained
    mixed = lax.psum_scatter(
        jnp.dot(picked, out_weight, preferred_element_type=jnp.float32).astype(jnp.bfloat16),
        "tp",
        scatter_dimension=0,
        tiled=True,
    ).astype(jnp.float32)
    own_rows = lax.dynamic_slice_in_dim(residual, lax.axis_index("tp") * quarter, quarter, 0)
    rows_mid = (own_rows.astype(jnp.float32) + mixed).astype(jnp.bfloat16)
    own_normed = row_norm(rows_mid.astype(jnp.float32), mlp_gain).astype(jnp.bfloat16)
    normed = lax.all_gather(own_normed, "tp", axis=0, tiled=True)
    gate = jnp.dot(
        normed,
        lax.all_gather(gate_weight, "sp", axis=0, tiled=True),
        preferred_element_type=jnp.float32,
    )
    upvals = jnp.dot(
        normed,
        lax.all_gather(up_weight, "sp", axis=0, tiled=True),
        preferred_element_type=jnp.float32,
    )
    full_down = lax.all_gather(down_weight, "sp", axis=1, tiled=True)
    hidden = (jax.nn.silu(gate) * upvals).astype(jnp.bfloat16)
    picked = hidden
    ffn = lax.psum_scatter(
        jnp.dot(picked, full_down, preferred_element_type=jnp.float32).astype(jnp.bfloat16),
        "tp",
        scatter_dimension=0,
        tiled=True,
    ).astype(jnp.float32)
    return (rows_mid.astype(jnp.float32) + ffn).astype(jnp.bfloat16)


def solution(mesh):
    return jax.shard_map(
        body,
        mesh=mesh,
        in_specs=(
            P("sp", "tp"),
            P("sp", "tp"),
            P("sp", "tp"),
            P("sp", "tp"),
            P("sp", "tp"),
            P("tp"),
            P("tp", None),
            P("sp", None),
            P(),
            P("sp", "tp"),
            P("sp", "tp"),
            P("tp", "sp"),
        ),
        out_specs=P(("sp", "tp"), None),
        check_vma=False,
    )
```

profile of v0, /device:TPU:0, one launch (start us, length us, event | category | flops | bytes accessed | tf_op | source)
XLA Modules:
  0.0 402.8 jit_solution(3665025626243340659)
XLA Ops:
  6.5 0.0 copy-start
  6.5 0.0 copy-start.2
  6.5 0.0 all-gather.13.cloned.1.call-start
  6.6 1.0 copy.56
  7.5 0.2 reduce_window_sum.13
  7.7 0.1 copy.61
  7.8 1.0 copy_bitcast_fusion
  8.7 0.0 copy-start.3
  8.7 0.0 copy-start.4
  8.8 1.0 copy_bitcast_fusion.1
  9.7 0.1 fusion.40
  9.8 0.1 broadcast_multiply_fusion
  9.9 0.3 fusion.38
  10.2 0.2 slice_negate_fusion
  10.4 0.1 bitcast_exponential_fusion
  10.5 1.2 fusion.19
  11.7 1.9 fusion.4
  13.6 0.0 all-gather.13.cloned.1.call-update
  13.6 0.0 reduce-scatter.3.cloned.1.call-start
  13.7 22.3 %all-gather = bf16[8,1,4]{2,1,0:T(2,128)(2,1)S(1)} all-gather(bf16[1,1,4]{2,1,0:T(2,128)(2,1)S(1)} %get-tuple-element.106), channel_id=2, replica_groups=mesh['sp'=8,'tp'=4] {'sp'}, dimensions={0}, use_global_device_ids=true | all-gather | bytes 72 | tf_op jit(solution)/shard_map/all_gather | solution.py:13
  35.9 0.1 copy.57
  36.0 0.1 copy.60
  36.1 0.1 copy.64
  36.2 0.0 copy-done.2
  36.2 0.4 convolution_bitcast_fusion.1
  36.6 20.1 %all-gather.13.cloned.1.call-done = bf16[32,128,128]{2,1,0:T(8,128)(2,1)} async-done(((bf16[4,128,128]{2,1,0:T(8,128)(2,1)}), bf16[32,128,128]{2,1,0:T(8,128)(2,1)}) %all-gather.13.cloned.1.call-update) | async-done | bytes 1048592 | tf_op jit(solution)/shard_map/all_gather | solution.py:13
  56.8 0.0 copy-start.1
  56.8 0.4 multiply_reduce_fusion
  57.2 0.1 copy.66
  57.4 0.1 copy.67
  57.5 0.2 mul.242
  57.7 0.0 copy-done
  57.7 0.0 copy-done.3
  57.7 0.0 copy-done.4
  57.7 1.3 convolution_convert_fusion
  59.0 0.0 reduce-scatter.3.cloned.1.call-update
  59.0 0.0 all-gather.7.cloned.1.call-start
  59.1 0.7 all-gather.7.cloned.1.call-update
  59.8 0.0 all-gather.11.cloned.1.call-start
  59.8 0.5 all-gather.11.cloned.1.call-update
  60.3 0.0 all-gather.9.cloned.1.call-start
  60.4 0.5 all-gather.9.cloned.1.call-update
  60.9 0.0 reduce-scatter.5.cloned.1.call-start
  61.0 26.0 %reduce-scatter.3.cloned.1.call-done = bf16[32,2048]{1,0:T(8,128)(2,1)} async-done(((bf16[128,2048]{1,0:T(8,128)(2,1)}), bf16[32,2048]{1,0:T(8,128)(2,1)}) %reduce-scatter.3.cloned.1.call-update) | async-done | bytes 131088 | tf_op jit(solution)/shard_map/reduce_scatter | solution.py:118
  87.0 1.1 fusion.10
  88.1 0.0 copy-done.1
  88.1 0.1 fusion.12
  88.2 6.6 %all_gather.22 = bf16[128,2048]{1,0:T(8,128)(2,1)S(1)} all-gather(bf16[32,2048]{1,0:T(8,128)(2,1)S(1)} %fusion.12), channel_id=1, replica_groups=mesh['sp'=8,'tp'=4] {'tp'}, dimensions={0}, use_global_device_ids=true | all-gather | bytes 655360 | tf_op jit(solution)/shard_map/all_gather | solution.py:127
  94.8 86.7 %all-gather.7.cloned.1.call-done = bf16[2048,1408]{1,0:T(8,128)(2,1)} async-done(((bf16[256,1408]{1,0:T(8,128)(2,1)}), bf16[2048,1408]{1,0:T(8,128)(2,1)}) %all-gather.7.cloned.1.call-update) | async-done | bytes 5767184 | tf_op jit(solution)/shard_map/all_gather | solution.py:130
  181.5 3.6 fusion.44
  185.1 89.6 %all-gather.11.cloned.1.call-done = bf16[1408,2048]{1,0:T(8,128)(2,1)} async-done(((bf16[1408,256]{1,0:T(8,128)(2,1)}), bf16[1408,2048]{1,0:T(8,128)(2,1)}) %all-gather.11.cloned.1.call-update) | async-done | bytes 5767184 | tf_op jit(solution)/shard_map/all_gather | solution.py:138
  274.7 92.6 %all-gather.9.cloned.1.call-done = bf16[2048,1408]{1,0:T(8,128)(2,1)} async-done(((bf16[256,1408]{1,0:T(8,128)(2,1)}), bf16[2048,1408]{1,0:T(8,128)(2,1)}) %all-gather.9.cloned.1.call-update) | async-done | bytes 5767184 | tf_op jit(solution)/shard_map/all_gather | solution.py:135
  367.3 7.1 %convolution_convert_fusion.1 = bf16[128,2048]{1,0:T(8,128)(2,1)} fusion(bf16[1408,2048]{1,0:T(8,128)(2,1)} %all-gather.11.cloned.1.call-done, bf16[128,2048]{1,0:T(8,128)(2,1)S(1)} %all_gather.22, bf16[2048,1408]{1,0:T(8,128)(2,1)} %all-gather.9.cloned.1.call-done, f32[128,1408]{1,0:T(8,128)S(1)} %fusion.44), kind=kOutput, calls=%fused_computation.5 | convolution fusion | flops 1477738496 | bytes 13303808 | tf_op jit(solution)/shard_map/dot_general | solution.py:142
  374.4 0.0 reduce-scatter.5.cloned.1.call-update
  374.4 20.0 %reduce-scatter.5.cloned.1.call-done = bf16[32,2048]{1,0:T(8,128)(2,1)} async-done(((bf16[128,2048]{1,0:T(8,128)(2,1)}), bf16[32,2048]{1,0:T(8,128)(2,1)}) %reduce-scatter.5.cloned.1.call-update) | async-done | bytes 131088 | tf_op jit(solution)/shard_map/reduce_scatter | solution.py:141
  394.4 1.6 fusion.13
  (9 shorter events, 0.1 us)
Async XLA Ops:
  6.5 51.2 %copy-start = (bf16[512,2048]{1,0:T(8,128)(2,1)S(1)}, bf16[512,2048]{1,0:T(8,128)(2,1)}, u32[]{:S(2)}) copy-start(bf16[512,2048]{1,0:T(8,128)(2,1)} %param.22) | copy-start | bytes 6291460
  6.5 29.7 %copy-start.2 = (bf16[128,512]{1,0:T(8,128)(2,1)S(1)}, bf16[128,512]{1,0:T(8,128)(2,1)}, u32[]{:S(2)}) copy-start(bf16[128,512]{1,0:T(8,128)(2,1)} %param.18) | copy-start | bytes 393220
  6.5 50.2 %all-gather.13.cloned.1.call-start = ((), (), s32[]{:S(2)}) async-start(), calls=%async_computation.7 | async-start | bytes 1179648 | tf_op jit(solution)/shard_map/all_gather | solution.py:13
  8.7 49.0 %copy-start.3 = (bf16[128,512]{1,0:T(8,128)(2,1)S(1)}, bf16[128,512]{1,0:T(8,128)(2,1)}, u32[]{:S(2)}) copy-start(bf16[128,512]{1,0:T(8,128)(2,1)} %param.19) | copy-start | bytes 393220
  8.7 49.0 %copy-start.4 = (f32[512]{0:T(512)S(1)}, f32[512]{0:T(512)}, u32[]{:S(2)}) copy-start(f32[512]{0:T(512)} %param.21) | copy-start | bytes 6148
  13.6 73.4 %reduce-scatter.3.cloned.1.call-start = ((), (), s32[]{:S(2)}) async-start(), calls=%async_computation.2 | async-start | bytes 655360 | tf_op jit(solution)/shard_map/reduce_scatter | solution.py:118
  56.8 31.3 %copy-start.1 = (f32[2048]{0:T(1024)S(1)}, f32[2048]{0:T(1024)}, u32[]{:S(2)}) copy-start(f32[2048]{0:T(1024)} %param.24) | copy-start | bytes 24580
  59.0 122.5 %all-gather.7.cloned.1.call-start = ((), (), s32[]{:S(2)}) async-start(), calls=%async_computation.3 | async-start | bytes 6488064 | tf_op jit(solution)/shard_map/all_gather | solution.py:130
  59.8 215.0 %all-gather.11.cloned.1.call-start = ((), (), s32[]{:S(2)}) async-start(), calls=%async_computation.5 | async-start | bytes 6488064 | tf_op jit(solution)/shard_map/all_gather | solution.py:138
  60.3 306.9 %all-gather.9.cloned.1.call-start = ((), (), s32[]{:S(2)}) async-start(), calls=%async_computation.4 | async-start | bytes 6488064 | tf_op jit(solution)/shard_map/all_gather | solution.py:135
  60.9 333.5 %reduce-scatter.5.cloned.1.call-start = ((), (), s32[]{:S(2)}) async-start(), calls=%async_computation.6 | async-start | bytes 655360 | tf_op jit(solution)/shard_map/reduce_scatter | solution.py:141
Sparse Core Ops, SparseCore 0:
  13.7 42.9 all-gather.12
  59.3 27.6 reduce-scatter.2
  89.2 92.2 all-gather.6
  183.4 91.2 all-gather.10
  276.8 90.4 all-gather.8
  374.5 19.8 reduce-scatter.4
where the time goes:
time: 403 us
  waiting for transfers between devices  337 us (84%)
  blocking collectives  28.9 us (7%)
  matrix products  14.6 us (4%)
  between operations  13.6 us (3%)
  other arithmetic  6.89 us (2%)
    all_gather x1, waiting for transfers between devices, body(): lax.all_gather(up_weight, 'sp', axis=0, tiled=True)  92.6 us
    all_gather x1, waiting for transfers between devices, body(): full_down = lax.all_gather(down_weight, 'sp', axis=1, tiled=True)  89.6 us
    all_gather x1, waiting for transfers between devices, body(): lax.all_gather(gate_weight, 'sp', axis=0, tiled=True)  86.7 us
    reduce_scatter x1, waiting for transfers between devices, body(): lax.psum_scatter(jnp.dot(picked, out_weight, preferred_element_type=jnp.f...  26 us
    all_gather x1, blocking collectives, prefix_2(): lax.all_gather(a.astype(kind), axis)  22.3 us
    all_gather x1, waiting for transfers between devices, prefix_2(): lax.all_gather(a.astype(kind), axis)  20.1 us
    reduce_scatter x1, waiting for transfers between devices, body(): lax.psum_scatter(jnp.dot(picked, full_down, preferred_element_type=jnp.fl...  20 us
  transfers between devices with their start and end apart: 6, of which 6 were waited for; matrix products, arithmetic and copies ran while one was open for 1% of the time, Pallas kernels for 0%

commit v1 on v0

--- a/solution.py
+++ b/solution.py
@@ -135,7 +135,12 @@
         lax.all_gather(up_weight, "sp", axis=0, tiled=True),
         preferred_element_type=jnp.float32,
     )
-    full_down = lax.all_gather(down_weight, "sp", axis=1, tiled=True)
+    ring = [down_weight]
+    for hop in range(7):
+        ring.append(lax.ppermute(ring[-1], "sp", [(dev, (dev + 1) % 8) for dev in range(8)]))
+    full_down = jnp.roll(
+        jnp.concatenate(ring[::-1], axis=1), (lax.axis_index("sp") + 1) * ring[0].shape[1], axis=1
+    )
     hidden = (jax.nn.silu(gate) * upvals).astype(jnp.bfloat16)
     picked = hidden
     ffn = lax.psum_scatter(

time: 403 us -> 371 us (0.921)
  waiting for transfers between devices: 337 us -> 270 us
  local copies, waits for them, and re-layouts: 1.78 us -> 28.5 us
    ppermute x0 -> x7, waiting for transfers between devices: none -> 184 us  [body(): lax.ppermute(ring[-1], 'sp', [(dev, (dev + 1) % 8) for dev in range(8)])]
    all_gather x1 -> x0, waiting for transfers between devices: 89.6 us -> none  [body(): full_down = lax.all_gather(down_weight, 'sp', axis=1, tiled=True)]
    all_gather x1, waiting for transfers between devices: 86.7 us -> 0.01 us  [body(): lax.all_gather(gate_weight, 'sp', axis=0, tiled=True)]
    all_gather x1, waiting for transfers between devices: 92.6 us -> 46.1 us  [body(): lax.all_gather(up_weight, 'sp', axis=0, tiled=True)]
    reduce_scatter x1, waiting for transfers between devices: 26 us -> 0.01 us  [body(): lax.psum_scatter(jnp.dot(picked, out_weight, preferred_element_type=jnp.f...]
    unnamed x10 -> x37, local copies, waits for them, and re-layouts: 0.03 us -> 25.2 us
  transfers between devices with their start and end apart: 6 -> 12, of which waited for: 6 -> 10; matrix products, arithmetic and copies ran while one was open for 1% -> 8% of each run, Pallas kernels for 0% -> 0%
where the time goes in v1:
time: 371 us; the launch traced here: 370 us
  waiting for transfers between devices  270 us (73%)
  blocking collectives  29.9 us (8%)
  local copies, waits for them, and re-layouts  28.5 us (8%)
  matrix products  18.5 us (5%)
  between operations  13.3 us (4%)
  other arithmetic  7.52 us (2%)
    ppermute x7, waiting for transfers between devices, body(): lax.ppermute(ring[-1], 'sp', [(dev, (dev + 1) % 8) for dev in range(8)])  184 us
    all_gather x1, waiting for transfers between devices, body(): lax.all_gather(up_weight, 'sp', axis=0, tiled=True)  46.1 us
    unnamed x37, local copies, waits for them, and re-layouts  25.2 us
    all_gather x1, blocking collectives, prefix_2(): lax.all_gather(a.astype(kind), axis)  22.3 us
    reduce_scatter x1, waiting for transfers between devices, body(): lax.psum_scatter(jnp.dot(picked, full_down, preferred_element_type=jnp.fl...  20 us
    all_gather x1, waiting for transfers between devices, prefix_2(): lax.all_gather(a.astype(kind), axis)  18.5 us
    all_gather x1, blocking collectives, body(): normed = lax.all_gather(own_normed, 'tp', axis=0, tiled=True)  7.64 us
  transfers between devices with their start and end apart: 12, of which 10 were waited for; matrix products, arithmetic and copies ran while one was open for 8% of the time, Pallas kernels for 0%

profile of v1, /device:TPU:0, one launch (start us, length us, event | category | flops | bytes accessed | tf_op | source)
XLA Modules:
  0.0 369.8 jit_solution(2066233924465787406)
XLA Ops:
  6.6 0.9 copy.56
  7.5 0.2 reduce_window_sum.13
  7.7 0.1 copy.61
  7.7 0.6 exponential_multiply_fusion
  8.3 0.9 copy_bitcast_fusion
  9.2 0.9 copy_bitcast_fusion.1
  10.2 0.1 fusion.45
  10.2 0.1 broadcast_multiply_fusion
  10.3 0.3 fusion.43
  10.7 0.2 slice_negate_fusion
  10.9 0.1 bitcast_exponential_fusion
  10.9 1.2 fusion.24
  12.1 1.9 fusion.9
  14.0 0.0 reduce-scatter.3.cloned.1.call-start
  14.1 22.3 %all-gather = bf16[8,1,4]{2,1,0:T(2,128)(2,1)S(1)} all-gather(bf16[1,1,4]{2,1,0:T(2,128)(2,1)S(1)} %get-tuple-element.106), channel_id=2, replica_groups=mesh['sp'=8,'tp'=4] {'sp'}, dimensions={0}, use_global_device_ids=true | all-gather | bytes 72 | tf_op jit(solution)/shard_map/all_gather | solution.py:13
  36.4 0.1 copy.57
  36.5 0.1 copy.60
  36.5 0.1 copy.64
  36.7 2.0 convolution_bitcast_fusion.1
  38.7 18.5 %all-gather.10.cloned.1.call-done = bf16[32,128,128]{2,1,0:T(8,128)(2,1)} async-done(((bf16[4,128,128]{2,1,0:T(8,128)(2,1)}), bf16[32,128,128]{2,1,0:T(8,128)(2,1)}) %all-gather.10.cloned.1.call-update) | async-done | bytes 1048592 | tf_op jit(solution)/shard_map/all_gather | solution.py:13
  57.2 1.4 multiply_reduce_fusion
  58.6 0.8 copy.67
  59.4 0.1 copy.66
  59.6 0.2 mul.245
  59.8 2.3 convolution_convert_fusion
  62.1 0.0 all-gather.6.cloned.1.call-start
  62.1 0.7 all-gather.6.cloned.1.call-update
  62.8 0.5 all-gather.8.cloned.1.call-update
  63.4 0.0 reduce-scatter.5.cloned.1.call-start
  63.4 1.7 collective-permute-start
  65.1 22.1 %collective-permute-done = bf16[1408,256]{1,0:T(8,128)(2,1)S(1)} collective-permute-done((bf16[1408,256]{1,0:T(8,128)(2,1)S(1)}, bf16[1408,256]{1,0:T(8,128)(2,1)S(1)}, u32[]{:S(2)}, u32[]{:S(2)}) %collective-permute-start) | collective-permute-done | bytes 720928 | tf_op jit(solution)/shard_map/ppermute | solution.py:140
  87.2 18.2 %collective-permute-done.1 = bf16[1408,256]{1,0:T(8,128)(2,1)S(1)} collective-permute-done((bf16[1408,256]{1,0:T(8,128)(2,1)S(1)}, bf16[1408,256]{1,0:T(8,128)(2,1)S(1)}, u32[]{:S(2)}, u32[]{:S(2)}) %collective-permute-start.1) | collective-permute-done | bytes 720928 | tf_op jit(solution)/shard_map/ppermute | solution.py:140
  105.4 0.9 copy-done.2
  106.3 35.7 %collective-permute-done.2 = bf16[1408,256]{1,0:T(8,128)(2,1)S(1)} collective-permute-done((bf16[1408,256]{1,0:T(8,128)(2,1)S(1)}, bf16[1408,256]{1,0:T(8,128)(2,1)S(1)}, u32[]{:S(2)}, u32[]{:S(2)}) %collective-permute-start.2) | collective-permute-done | bytes 720928 | tf_op jit(solution)/shard_map/ppermute | solution.py:140
  142.0 0.9 copy-done.4
  142.9 29.4 %collective-permute-done.3 = bf16[1408,256]{1,0:T(8,128)(2,1)S(1)} collective-permute-done((bf16[1408,256]{1,0:T(8,128)(2,1)S(1)}, bf16[1408,256]{1,0:T(8,128)(2,1)S(1)}, u32[]{:S(2)}, u32[]{:S(2)}) %collective-permute-start.3) | collective-permute-done | bytes 720928 | tf_op jit(solution)/shard_map/ppermute | solution.py:140
  172.3 0.9 copy-done.6
  173.2 35.3 %collective-permute-done.4 = bf16[1408,256]{1,0:T(8,128)(2,1)} collective-permute-done((bf16[1408,256]{1,0:T(8,128)(2,1)S(1)}, bf16[1408,256]{1,0:T(8,128)(2,1)}, u32[]{:S(2)}, u32[]{:S(2)}) %collective-permute-start.4) | collective-permute-done | bytes 720928 | tf_op jit(solution)/shard_map/ppermute | solution.py:140
  208.6 1.3 fusion.15
  209.9 30.7 %collective-permute-done.5 = bf16[1408,256]{1,0:T(8,128)(2,1)} collective-permute-done((bf16[1408,256]{1,0:T(8,128)(2,1)}, bf16[1408,256]{1,0:T(8,128)(2,1)}, u32[]{:S(2)}, u32[]{:S(2)}) %collective-permute-start.5) | collective-permute-done | bytes 720928 | tf_op jit(solution)/shard_map/ppermute | solution.py:140
  240.6 0.1 fusion.17
  240.7 7.6 %all_gather.19 = bf16[128,2048]{1,0:T(8,128)(2,1)} all-gather(bf16[32,2048]{1,0:T(8,128)(2,1)S(1)} %fusion.17), channel_id=1, replica_groups=mesh['sp'=8,'tp'=4] {'tp'}, dimensions={0}, use_global_device_ids=true | all-gather | bytes 655360 | tf_op jit(solution)/shard_map/all_gather | solution.py:127
  248.3 12.7 %collective-permute-done.6 = bf16[1408,256]{1,0:T(8,128)(2,1)S(1)} collective-permute-done((bf16[1408,256]{1,0:T(8,128)(2,1)}, bf16[1408,256]{1,0:T(8,128)(2,1)S(1)}, u32[]{:S(2)}, u32[]{:S(2)}) %collective-permute-start.6) | collective-permute-done | bytes 720928 | tf_op jit(solution)/shard_map/ppermute | solution.py:140
  261.1 1.0 constant_dynamic-update-slice_fusion.15
  262.0 2.1 constant_dynamic-update-slice_fusion.14
  264.1 2.1 constant_dynamic-update-slice_fusion.13
  266.2 2.1 constant_dynamic-update-slice_fusion.12
  268.3 2.1 constant_dynamic-update-slice_fusion.11
  270.4 2.1 constant_dynamic-update-slice_fusion.10
  272.5 1.0 constant_dynamic-update-slice_fusion.9
  273.5 1.0 constant_dynamic-update-slice_fusion.8
  274.5 1.0 constant_dynamic-update-slice_fusion.7
  275.5 2.1 constant_dynamic-update-slice_fusion.6
  277.6 2.1 constant_dynamic-update-slice_fusion.5
  279.7 1.0 constant_dynamic-update-slice_fusion.4
  280.6 1.0 constant_dynamic-update-slice_fusion.3
  281.6 1.0 constant_dynamic-update-slice_fusion.2
  282.6 1.0 constant_dynamic-update-slice_fusion.1
  283.5 0.9 constant_dynamic-update-slice_fusion
  284.5 3.8 %fusion.50 = f32[128,1408]{1,0:T(8,128)S(1)} fusion(bf16[128,2048]{1,0:T(8,128)(2,1)} %all_gather.19, bf16[2048,1408]{1,0:T(8,128)(2,1)} %all-gather.6.cloned.1.call-done), kind=kOutput, calls=%fused_computation.101 | convolution fusion | flops 738197504 | bytes 7012352 | tf_op jit(solution)/shard_map/dot_general | solution.py:128
  288.3 46.1 %all-gather.8.cloned.1.call-done = bf16[2048,1408]{1,0:T(8,128)(2,1)} async-done(((bf16[256,1408]{1,0:T(8,128)(2,1)}), bf16[2048,1408]{1,0:T(8,128)(2,1)}) %all-gather.8.cloned.1.call-update) | async-done | bytes 5767184 | tf_op jit(solution)/shard_map/all_gather | solution.py:135
  334.4 7.2 %fusion.3 = bf16[128,2048]{1,0:T(8,128)(2,1)} fusion(bf16[1408,4096]{1,0:T(8,128)(2,1)} %constant_dynamic-update-slice_fusion, s32[]{:T(128)S(6)} %select_n.38, bf16[128,2048]{1,0:T(8,128)(2,1)} %all_gather.19, bf16[2048,1408]{1,0:T(8,128)(2,1)} %all-gather.8.cloned.1.call-done, f32[128,1408]{1,0:T(8,128)S(1)} %fusion.50), kind=kOutput, calls=%fused_computation.6 | convolution fusion | flops 1477738496 | bytes 13303812 | tf_op jit(solution)/shard_map/dot_general | solution.py:147
  341.6 20.0 %reduce-scatter.5.cloned.1.call-done = bf16[32,2048]{1,0:T(8,128)(2,1)} async-done(((bf16[128,2048]{1,0:T(8,128)(2,1)}), bf16[32,2048]{1,0:T(8,128)(2,1)}) %reduce-scatter.5.cloned.1.call-update) | async-done | bytes 131088 | tf_op jit(solution)/shard_map/reduce_scatter | solution.py:146
  361.7 1.6 fusion.18
  (40 shorter events, 0.2 us)
Async XLA Ops:
  6.5 53.2 %copy-start = (bf16[512,2048]{1,0:T(8,128)(2,1)S(1)}, bf16[512,2048]{1,0:T(8,128)(2,1)}, u32[]{:S(2)}) copy-start(bf16[512,2048]{1,0:T(8,128)(2,1)} %param.22) | copy-start | bytes 6291460
  6.5 56.9 %copy-start.1 = (bf16[1408,256]{1,0:T(8,128)(2,1)S(1)}, bf16[1408,256]{1,0:T(8,128)(2,1)}, u32[]{:S(2)}) copy-start(bf16[1408,256]{1,0:T(8,128)(2,1)} %param.27) | copy-start | bytes 2162692
  6.5 234.0 %copy-start.10 = (f32[2048]{0:T(1024)S(1)}, f32[2048]{0:T(1024)}, u32[]{:S(2)}) copy-start(f32[2048]{0:T(1024)} %param.24) | copy-start | bytes 24580
  6.5 50.7 %all-gather.10.cloned.1.call-start = ((), (), s32[]{:S(2)}) async-start(), calls=%async_computation.6 | async-start | bytes 1179648 | tf_op jit(solution)/shard_map/all_gather | solution.py:13
  14.0 194.5 %reduce-scatter.3.cloned.1.call-start = ((), (), s32[]{:S(2)}) async-start(), calls=%async_computation.2 | async-start | bytes 655360 | tf_op jit(solution)/shard_map/reduce_scatter | solution.py:118
  62.1 222.4 %all-gather.6.cloned.1.call-start = ((), (), s32[]{:S(2)}) async-start(), calls=%async_computation.3 | async-start | bytes 6488064 | tf_op jit(solution)/shard_map/all_gather | solution.py:130
  62.8 271.6 %all-gather.8.cloned.1.call-start = ((), (), s32[]{:S(2)}) async-start(), calls=%async_computation.4 | async-start | bytes 6488064 | tf_op jit(solution)/shard_map/all_gather | solution.py:135
  63.4 298.3 %reduce-scatter.5.cloned.1.call-start = ((), (), s32[]{:S(2)}) async-start(), calls=%async_computation.5 | async-start | bytes 655360 | tf_op jit(solution)/shard_map/reduce_scatter | solution.py:146
  63.4 23.8 %collective-permute-start = (bf16[1408,256]{1,0:T(8,128)(2,1)S(1)}, bf16[1408,256]{1,0:T(8,128)(2,1)S(1)}, u32[]{:S(2)}, u32[]{:S(2)}) collective-permute-start(bf16[1408,256]{1,0:T(8,128)(2,1)S(1)} %copy-done.1), channel_id=1, source_target_pairs={{0,4},{4,8},{8,12},{12,16},{16,20},{20,24},{24,28},{28,0},{1,5},{5... | collective-permute-start | bytes 2162696 | tf_op jit(solution)/shard_map/ppermute | solution.py:140
  87.2 18.2 %collective-permute-start.1 = (bf16[1408,256]{1,0:T(8,128)(2,1)S(1)}, bf16[1408,256]{1,0:T(8,128)(2,1)S(1)}, u32[]{:S(2)}, u32[]{:S(2)}) collective-permute-start(bf16[1408,256]{1,0:T(8,128)(2,1)S(1)} %collective-permute-done), channel_id=1, source_target_pairs={{0,4},{4,8},{8,12},{12,16},{16,20},{20,24},{24,28},{28,0},{1,5},{5... | collective-permute-start | bytes 2162696 | tf_op jit(solution)/shard_map/ppermute | solution.py:140
  105.4 0.9 copy-start.2
  106.3 35.7 %collective-permute-start.2 = (bf16[1408,256]{1,0:T(8,128)(2,1)S(1)}, bf16[1408,256]{1,0:T(8,128)(2,1)S(1)}, u32[]{:S(2)}, u32[]{:S(2)}) collective-permute-start(bf16[1408,256]{1,0:T(8,128)(2,1)S(1)} %collective-permute-done.1), channel_id=1, source_target_pairs={{0,4},{4,8},{8,12},{12,16},{16,20},{20,24},{24,28},{28,0},{1,5},{5... | collective-permute-start | bytes 2162696 | tf_op jit(solution)/shard_map/ppermute | solution.py:140
  142.0 0.9 copy-start.4
  142.9 29.4 %collective-permute-start.3 = (bf16[1408,256]{1,0:T(8,128)(2,1)S(1)}, bf16[1408,256]{1,0:T(8,128)(2,1)S(1)}, u32[]{:S(2)}, u32[]{:S(2)}) collective-permute-start(bf16[1408,256]{1,0:T(8,128)(2,1)S(1)} %collective-permute-done.2), channel_id=1, source_target_pairs={{0,4},{4,8},{8,12},{12,16},{16,20},{20,24},{24,28},{28,0},{1,5},{5... | collective-permute-start | bytes 2162696 | tf_op jit(solution)/shard_map/ppermute | solution.py:140
  172.3 0.9 copy-start.6
  173.2 35.4 %collective-permute-start.4 = (bf16[1408,256]{1,0:T(8,128)(2,1)S(1)}, bf16[1408,256]{1,0:T(8,128)(2,1)}, u32[]{:S(2)}, u32[]{:S(2)}) collective-permute-start(bf16[1408,256]{1,0:T(8,128)(2,1)S(1)} %collective-permute-done.3), channel_id=1, source_target_pairs={{0,4},{4,8},{8,12},{12,16},{16,20},{20,24},{24,28},{28,0},{1,5},{5... | collective-permute-start | bytes 2162696 | tf_op jit(solution)/shard_map/ppermute | solution.py:140
  208.6 32.0 %collective-permute-start.5 = (bf16[1408,256]{1,0:T(8,128)(2,1)}, bf16[1408,256]{1,0:T(8,128)(2,1)}, u32[]{:S(2)}, u32[]{:S(2)}) collective-permute-start(bf16[1408,256]{1,0:T(8,128)(2,1)} %collective-permute-done.4), channel_id=1, source_target_pairs={{0,4},{4,8},{8,12},{12,16},{16,20},{20,24},{24,28},{28,0},{1,5},{5... | collective-permute-start | bytes 2162696 | tf_op jit(solution)/shard_map/ppermute | solution.py:140
  208.6 71.1 %copy-start.7 = (bf16[1408,256]{1,0:T(8,128)(2,1)S(1)}, bf16[1408,256]{1,0:T(8,128)(2,1)}, u32[]{:S(2)}) copy-start(bf16[1408,256]{1,0:T(8,128)(2,1)} %copy-done.6) | copy-start | bytes 2162692
  208.6 72.0 %copy-start.5 = (bf16[1408,256]{1,0:T(8,128)(2,1)S(1)}, bf16[1408,256]{1,0:T(8,128)(2,1)}, u32[]{:S(2)}) copy-start(bf16[1408,256]{1,0:T(8,128)(2,1)} %copy-done.4) | copy-start | bytes 2162692
  208.6 73.0 %copy-start.3 = (bf16[1408,256]{1,0:T(8,128)(2,1)S(1)}, bf16[1408,256]{1,0:T(8,128)(2,1)}, u32[]{:S(2)}) copy-start(bf16[1408,256]{1,0:T(8,128)(2,1)} %copy-done.2) | copy-start | bytes 2162692
  209.9 30.8 %copy-start.8 = (bf16[32,2048]{1,0:T(8,128)(2,1)}, bf16[32,2048]{1,0:T(8,128)(2,1)S(1)}, u32[]{:S(2)}) copy-start(bf16[32,2048]{1,0:T(8,128)(2,1)S(1)} %get-tuple-element.98) | copy-start | bytes 393220
  240.6 20.5 %collective-permute-start.6 = (bf16[1408,256]{1,0:T(8,128)(2,1)}, bf16[1408,256]{1,0:T(8,128)(2,1)S(1)}, u32[]{:S(2)}, u32[]{:S(2)}) collective-permute-start(bf16[1408,256]{1,0:T(8,128)(2,1)} %collective-permute-done.5), channel_id=1, source_target_pairs={{0,4},{4,8},{8,12},{12,16},{16,20},{20,24},{24,28},{28,0},{1,5},{5... | collective-permute-start | bytes 2162696 | tf_op jit(solution)/shard_map/ppermute | solution.py:140
  283.5 78.1 %copy-start.9 = (bf16[32,2048]{1,0:T(8,128)(2,1)S(1)}, bf16[32,2048]{1,0:T(8,128)(2,1)}, u32[]{:S(2)}) copy-start(bf16[32,2048]{1,0:T(8,128)(2,1)} %copy-done.8) | copy-start | bytes 393220
Sparse Core Ops, SparseCore 0:
  14.2 42.9 all-gather.9
  62.2 27.7 reduce-scatter.2
  92.2 133.9 all-gather.5
  228.2 106.1 all-gather.7
  341.8 19.8 reduce-scatter.4
